TPU v7x, 256 devices: a 4x2x16 block of a 4x16x16 slice. The times are simulated.
256 devices in a mesh: grp: 2 (over y), sp: 16 (over z), tp: 8 (over x, core).
Axes of the slice: x: 4, y: 2, z: 16, core: 2. Of those that a mesh axis runs over, the one named last changes fastest.
The devices are a block of a 4x16x16 slice.
Arguments:
- tokens: bfloat16 [2, 16384, 2048], P('grp', ('sp', 'tp')), parts along dimension 0, may hold values from -6 to 6
- norm_gain: bfloat16 [2048], replicated, may hold values from 0.099609375 to 1.8984375
- w_query: bfloat16 [2048, 1024], P('sp'), may hold values from -0.125 to 0.125
- w_forget: bfloat16 [2048, 1024], P('sp'), may hold values from -0.125 to 0.125
- w_input: bfloat16 [2048, 1024], P('sp'), may hold values from -0.125 to 0.125
- floor_gap: float32 [1024], replicated, may hold values from 1.8310547e-05 to 0.12
- extra_decay: float32 [2, 16384, 16], P('grp', ('sp', 'tp')), parts along dimension 0, may hold values from -1.4 to 0, as said below
- init_state: float32 [2, 16, 64, 64], P('grp'), parts along dimension 0, may hold values from -0.03125 to 0.03125
- head_norm_gain: bfloat16 [1024], replicated, may hold values from 0.099609375 to 1.8984375
- w_output: bfloat16 [1024, 2048], P(None, 'sp'), may hold values from -0.1875 to 0.1875
Outputs:
- mixed: bfloat16 [2, 16384, 2048], P('grp', ('sp', 'tp')), parts along dimension 0
- final_state: float32 [2, 65536], P('grp', ('sp', 'tp')), parts along dimension 0
There are 2 independent parts, one for each index of `grp`. A program takes and returns all parts, laid end to end along the dimension named above; an argument that names none is the same for every part. Nothing has to cross between parts.
Inputs may be any that keep to these rules, and one draw needn't show every extreme that they name: `extra_decay`: no entry is positive.
All inputs are finite; a program needn't handle non-finite values.
Results may differ from a plain program's by a relative error of at most 0.014.
Values may be sent and summed in bfloat16 or wider, within the bound.
A program may use at most 128 MiB of HBM per device.

v0:
```python
import jax
import jax.numpy as jnp
from jax import lax
from jax.sharding import Mesh
from jax.sharding import PartitionSpec as P

HEADS = 16
HEAD = 64
BLOCK = 64
SP_TP = ("sp", "tp_0", "tp_1")
EPSILON = 1e-05


def nothing_yet(value, identity):
    return jax.tree.map(
        lambda a, e: jnp.broadcast_to(jnp.asarray(e, a.dtype), a.shape), value, identity
    )


def entering_2(value, axes, combine, identity):
    before = start = nothing_yet(value, identity)
    total = value
    for axis in reversed(axes):
        peers, mine = (lax.axis_size(axis), lax.axis_index(axis))
        pieces = jax.tree.map(
            lambda part, kind: lax.all_gather(part.astype(kind), axis),
            total,
            (jnp.bfloat16, jnp.bfloat16),
        )
        inside, total = (start, start)
        for k in range(peers):
            passed = k < mine
            total = combine(
                total, jax.tree.map(lambda part, own: part[k].astype(own.dtype), pieces, value)
            )
            inside = jax.tree.map(lambda new, old: jnp.where(passed, new, old), total, inside)
        before = combine(inside, before)
    return before


def prefix_by_axis(value, axes, combine, identity):
    before = start = nothing_yet(value, identity)
    total = value
    for axis in reversed(axes):
        peers, mine = (lax.axis_size(axis), lax.axis_index(axis))
        pieces = lax.all_gather(total, axis)
        inside, total = (start, start)
        for k in reversed(range(peers)):
            passed = k > mine
            total = combine(total, pieces[k])
            inside = jnp.where(passed, total, inside)
        before = combine(inside, before)
    return before


def reduced_to_own(pieces, axes, order):
    inside = pieces.shape[1:]
    pieces = pieces.reshape(*(lax.axis_size(a) for a in axes), *inside)
    pieces = jnp.moveaxis(pieces, order, range(len(axes))).reshape(-1, *inside)
    for k in order:
        pieces = lax.psum_scatter(pieces, axes[k], scatter_dimension=0, tiled=True)
    return pieces[0]


def in_blocks(value, dim, peers):
    lengths = value.shape
    pieces = value.reshape(*lengths[:dim], peers, lengths[dim] // peers, *lengths[dim + 1 :])
    return jnp.moveaxis(pieces, dim, 0)


def summed_rows(value, axes, order, dim):
    peers = lax.axis_size(axes)
    return reduced_to_own(in_blocks(value, dim, peers), axes, order)


def layer_normed(tokens, norm_gain):
    values = tokens.astype(jnp.float32)
    center = values - jnp.mean(values, axis=-1, keepdims=True)
    spread = jnp.mean(center * center, axis=-1, keepdims=True)
    return (center * lax.rsqrt(spread + EPSILON) * norm_gain.astype(jnp.float32)).astype(
        jnp.bfloat16
    )


def gate_terms(query_sum, forget_sum, input_sum, floor_gap, extra_decay):
    query_raw = query_sum.astype(jnp.bfloat16)
    forget_raw = forget_sum.astype(jnp.bfloat16)
    input_raw = input_sum.astype(jnp.bfloat16)
    forget_pre = forget_raw.astype(jnp.float32)
    split_shape = forget_pre.shape[:-1] + (HEADS, HEAD)
    log_keep = jnp.logaddexp(
        jnp.log1p(-floor_gap), jnp.log(floor_gap) + jax.nn.log_sigmoid(forget_pre)
    )
    log_keep = log_keep.reshape(split_shape) + extra_decay[..., None]
    key_gate = (floor_gap * jax.nn.sigmoid(-forget_pre)).reshape(split_shape)
    query = jax.nn.silu(query_raw.astype(jnp.float32)).reshape(split_shape)
    values = input_raw.astype(jnp.float32).reshape(split_shape)
    return (query, key_gate, values, log_keep)


def block_pass(query, key_gate, values, log_keep):
    highest = lax.Precision.HIGHEST
    cumul = jnp.cumsum(log_keep, axis=2)
    q_decayed = query * jnp.exp(cumul)
    key_decayed = key_gate * jnp.exp(-cumul)
    causal = lax.broadcasted_iota(jnp.int32, (BLOCK, BLOCK), 0) >= lax.broadcasted_iota(
        jnp.int32, (BLOCK, BLOCK), 1
    )
    scores = jnp.einsum("snthd,snuhd->snhtu", q_decayed, key_decayed, precision=highest)
    scores = jnp.where(causal, scores, 0.0)
    within = jnp.einsum("snhtu,snuhe->snthe", scores, values, precision=highest)
    totals = cumul[:, :, -1]
    k_tail = key_gate * jnp.exp(totals[:, :, None] - cumul)
    block_state = jnp.einsum("snthd,snthe->snhde", k_tail, values, precision=highest)
    return (q_decayed, within, totals, block_state)


def linked_advance(earlier, later):
    return (earlier[0] + later[0], jnp.exp(later[0])[..., None] * earlier[1] + later[1])


def add_logs(earlier, later):
    return earlier + later


def read_out(q_global, leading_logarithm, prefix_state, init_part):
    carried = jnp.exp(leading_logarithm)[..., None] * init_part + prefix_state
    added = jnp.einsum("snthd,shde->snthe", q_global, carried, precision=lax.Precision.HIGHEST)
    return (carried, added)


def body(
    tokens,
    norm_gain,
    w_query,
    w_forget,
    w_input,
    floor_gap,
    extra_decay,
    init_state,
    head_norm_gain,
    w_output,
):
    normed = layer_normed(tokens, norm_gain)
    seqs, span = (tokens.shape[0], tokens.shape[1])

    def add_rows(piece):
        return jnp.dot(normed, piece, preferred_element_type=jnp.float32)

    query_sum = add_rows(lax.all_gather(w_query, "sp", axis=0, tiled=True))
    forget_sum = add_rows(lax.all_gather(w_forget, "sp", axis=0, tiled=True))
    input_sum = add_rows(lax.all_gather(w_input, "sp", axis=0, tiled=True))
    query, key_gate, values, log_keep = gate_terms(
        query_sum, forget_sum, input_sum, floor_gap, extra_decay
    )
    blocks = span // BLOCK
    blocked = (seqs, blocks, BLOCK, HEADS, HEAD)
    q_decayed, within, totals, block_state = block_pass(
        query.reshape(blocked),
        key_gate.reshape(blocked),
        values.reshape(blocked),
        log_keep.reshape(blocked),
    )
    running_state = jnp.zeros((seqs, HEADS, HEAD, HEAD), jnp.float32)
    running_log = jnp.zeros((seqs, HEADS, HEAD), jnp.float32)
    entering_list = []
    offset_list = []
    for number in range(blocks):
        entering_list.append(running_state)
        offset_list.append(running_log)
        running_state = (
            jnp.exp(totals[:, number])[..., None] * running_state + block_state[:, number]
        )
        running_log = running_log + totals[:, number]
    entering = jnp.stack(entering_list, axis=1)
    offsets = jnp.stack(offset_list, axis=1)
    local_out = within + jnp.einsum(
        "snthd,snhde->snthe", q_decayed, entering, precision=lax.Precision.HIGHEST
    )
    q_global = q_decayed * jnp.exp(offsets[:, :, None])
    leading_logarithm, prefix_state = entering_2(
        (running_log, running_state),
        SP_TP,
        linked_advance,
        (jnp.zeros_like(running_log), jnp.zeros_like(running_state)),
    )
    carried, added = read_out(q_global, leading_logarithm, prefix_state, init_state)
    flat_total = HEADS * HEAD * HEAD
    piece_count = flat_total // lax.axis_size(SP_TP)
    piece_start = lax.axis_index(SP_TP) * piece_count
    later_log = prefix_by_axis(running_log, SP_TP, add_logs, jnp.zeros_like(running_log))
    surviving = (jnp.exp(later_log)[..., None] * running_state).reshape(seqs, flat_total)
    summed = summed_rows(surviving.astype(jnp.bfloat16), SP_TP, (2, 0, 1), 1).astype(jnp.float32)
    initial_part = (
        jnp.exp(leading_logarithm + running_log + later_log)[..., None] * init_state
    ).reshape(seqs, flat_total)
    final_state = lax.dynamic_slice_in_dim(initial_part, piece_start, piece_count, 1) + summed
    recurrent = (local_out + added).reshape(seqs, span, HEADS, HEAD)
    average_power = jnp.mean(recurrent * recurrent, axis=-1, keepdims=True)
    scaled = (
        recurrent
        * lax.rsqrt(average_power + EPSILON)
        * head_norm_gain.astype(jnp.float32).reshape(HEADS, HEAD)
    )
    gated = scaled.reshape(seqs, span, HEADS * HEAD).astype(jnp.bfloat16)
    mixed = jnp.dot(
        gated,
        lax.all_gather(w_output, "sp", axis=1, tiled=True),
        preferred_element_type=jnp.float32,
    ).astype(jnp.bfloat16)
    return (mixed, final_state)


def solution(mesh):
    torus = Mesh(
        mesh.devices.reshape(mesh.shape["grp"], mesh.shape["sp"], 4, 2),
        ("grp", "sp", "tp_0", "tp_1"),
    )
    in_specs = (
        P("grp", SP_TP, None),
        P(),
        P("sp", None),
        P("sp", None),
        P("sp", None),
        P(),
        P("grp", SP_TP, None),
        P("grp", None, None, None),
        P(),
        P(None, "sp"),
    )
    out_specs = (P("grp", SP_TP, None), P("grp", SP_TP))
    return jax.shard_map(body, mesh=torus, in_specs=in_specs, out_specs=out_specs, check_vma=False)
```

profile of v0, /device:TPU:36, one launch (start us, length us, event | category | flops | bytes accessed | tf_op | source)
XLA Modules:
  0.0 588.2 jit_solution(18242492222280507001)
XLA Ops:
  14.5 85.1 %all-gather.10.cloned.1.call-done = bf16[2048,1024]{1,0:T(8,128)(2,1)} async-done(((bf16[128,1024]{1,0:T(8,128)(2,1)}), bf16[2048,1024]{1,0:T(8,128)(2,1)}) %all-gather.10.cloned.1.call-update) | async-done | bytes 4194320 | tf_op jit(solution)/shard_map/all_gather | solution.py:151
  99.6 3.8 add_select_fusion
  104.2 1.9 all_gather.51
  106.1 1.9 all_gather.58
  108.5 10.8 %all_gather.52 = bf16[4,1,16,64]{3,2,1,0:T(8,128)(2,1)S(1)} all-gather(bf16[1,1,16,64]{3,2,1,0:T(8,128)(2,1)S(1)} %get-tuple-element.47), channel_id=1, replica_groups=mesh['grp'=2,'sp'=16,'tp_0'=4,'tp_1'=2] {'tp_0'}, dimensions={0}, use_global_device_ids=true | all-gather | bytes 10240 | tf_op jit(solution)/shard_map/all_gather | solution.py:26
  119.4 11.9 %all_gather.59 = f32[4,1,16,64]{3,2,1,0:T(8,128)S(1)} all-gather(f32[1,1,16,64]{3,2,1,0:T(8,128)S(1)} %slice_add_fusion.18), channel_id=1, replica_groups=mesh['grp'=2,'sp'=16,'tp_0'=4,'tp_1'=2] {'tp_0'}, dimensions={0}, use_global_device_ids=true | all-gather | bytes 20480 | tf_op jit(solution)/shard_map/all_gather | solution.py:46
  131.3 29.1 %all_gather.53 = bf16[16,1,16,64]{3,2,1,0:T(8,128)(2,1)S(1)} all-gather(bf16[1,1,16,64]{3,2,1,0:T(8,128)(2,1)S(1)} %get-tuple-element.37), channel_id=1, replica_groups=mesh['grp'=2,'sp'=16,'tp_0'=4,'tp_1'=2] {'sp'}, dimensions={0}, use_global_device_ids=true | all-gather | bytes 34816 | tf_op jit(solution)/shard_map/all_gather | solution.py:26
  160.4 26.9 %all_gather.60 = f32[16,1,16,64]{3,2,1,0:T(8,128)S(1)} all-gather(f32[1,1,16,64]{3,2,1,0:T(8,128)S(1)} %slice_add_fusion.15), channel_id=1, replica_groups=mesh['grp'=2,'sp'=16,'tp_0'=4,'tp_1'=2] {'sp'}, dimensions={0}, use_global_device_ids=true | all-gather | bytes 69632 | tf_op jit(solution)/shard_map/all_gather | solution.py:46
  189.7 3.1 divide_multiply_fusion.1
  194.0 55.5 %all-gather.6.cloned.1.call-done = bf16[2048,1024]{1,0:T(8,128)(2,1)} async-done(((bf16[128,1024]{1,0:T(8,128)(2,1)}), bf16[2048,1024]{1,0:T(8,128)(2,1)}) %all-gather.6.cloned.1.call-update) | async-done | bytes 4194320 | tf_op jit(solution)/shard_map/all_gather | solution.py:152
  249.5 3.0 convolution_convert_fusion.3
  252.8 3.3 fusion.16
  263.6 2.6 all_gather.54
  266.6 14.0 %all_gather.55 = bf16[4,1,16,64,64]{4,3,2,1,0:T(8,128)(2,1)} all-gather(bf16[1,1,16,64,64]{4,3,2,1,0:T(8,128)(2,1)S(1)} %fusion.36), channel_id=1, replica_groups=mesh['grp'=2,'sp'=16,'tp_0'=4,'tp_1'=2] {'tp_0'}, dimensions={0}, use_global_device_ids=true | all-gather | bytes 655360 | tf_op jit(solution)/shard_map/all_gather | solution.py:26
  280.7 2.5 fusion.52
  287.2 2.0 broadcast_multiply_fusion.1
  291.8 2.4 convolution_select_fusion
  295.3 3.0 fusion.1
  298.3 114.6 %all-reduce.6.cloned.1.call-done = bf16[64,1,512]{2,0,1:T(8,128)(2,1)} async-done(((bf16[64,1,512]{2,0,1:T(8,128)(2,1)}), bf16[64,1,512]{2,0,1:T(8,128)(2,1)}) %all-reduce.6.cloned.1.call-update) | async-done | bytes 65552
  413.6 8.3 %all-reduce.3 = bf16[4,1,512]{2,0,1:T(4,128)(2,1)S(1)} all-reduce(bf16[4,1,512]{2,0,1:T(4,128)(2,1)S(1)} %constant_dynamic-slice_fusion), channel_id=4, replica_groups=mesh['grp'=2,'sp'=16,'tp_0'=4,'tp_1'=2] {'tp_0'}, use_global_device_ids=true, to_apply=%region_6.7.clone | all-reduce | flops 2048 | bytes 8192
  423.1 63.5 %all-gather.12.cloned.1.call-done = bf16[16,1,16,64,64]{4,3,2,1,0:T(8,128)(2,1)} async-done(((bf16[1,1,16,64,64]{4,3,2,1,0:T(8,128)(2,1)}), bf16[16,1,16,64,64]{4,3,2,1,0:T(8,128)(2,1)}) %all-gather.12.cloned.1.call-update) | async-done | bytes 2097168 | tf_op jit(solution)/shard_map/all_gather | solution.py:26
  486.6 10.3 %multiply_reduce_fusion = (f32[2,64,16]{1,2,0:T(8,128)S(1)}, f32[1,2,64,16,64]{2,4,3,1,0:T(8,128)}) fusion(f32[1,2,64,16,64]{2,4,3,1,0:T(8,128)} %fusion.1, f32[2,64,16,64]{3,2,1,0:T(8,128)S(1)} %copy-done.3, f32[1,16,64,64]{3,2,1,0:T(8,128)} %param.17, bf16[16,1,16,64,64]{4,3,2,1,0:T(8,128)(2,1)} %all-gather.12.cloned.1.call-done, ...), kind=kOutput, calls=%fused_computation.33 | convolution fusion | flops 107018240 | bytes 4829206 | tf_op jit(solution)/shard_map/snthd,shde->snthe/dot_general | solution.py:128
  499.4 78.2 %all-gather.14.cloned.1.call-done = bf16[1024,2048]{1,0:T(8,128)(2,1)} async-done(((bf16[1024,128]{1,0:T(8,128)(2,1)}), bf16[1024,2048]{1,0:T(8,128)(2,1)}) %all-gather.14.cloned.1.call-update) | async-done | bytes 4194320 | tf_op jit(solution)/shard_map/all_gather | solution.py:208
  577.6 3.7 fusion
  (104 shorter events, 31.6 us)
Async XLA Ops:
  7.2 92.5 %all-gather.10.cloned.1.call-start = ((), (), s32[]{:S(2)}) async-start(), calls=%async_computation.3 | async-start | bytes 4456448 | tf_op jit(solution)/shard_map/all_gather | solution.py:151
  8.0 181.7 %all-gather.8.cloned.1.call-start = ((), (), s32[]{:S(2)}) async-start(), calls=%async_computation.2 | async-start | bytes 4456448 | tf_op jit(solution)/shard_map/all_gather | solution.py:150
  8.8 240.7 %all-gather.6.cloned.1.call-start = ((), (), s32[]{:S(2)}) async-start(), calls=%async_computation.1 | async-start | bytes 4456448 | tf_op jit(solution)/shard_map/all_gather | solution.py:152
  9.6 271.0 %reduce-scatter.4.cloned.1.call-start = ((), (), s32[]{:S(2)}) async-start(), calls=%async_computation.6 | async-start | bytes 196608 | tf_op jit(solution)/shard_map/reduce_scatter | solution.py:61
  10.4 93.0 %copy-start.9 = (f32[2048]{0:T(1024)}, f32[2048]{0:T(1024)S(1)}, u32[]{:S(2)}) copy-start(f32[2048]{0:T(1024)S(1)} %convert_element_type.904) | copy-start | bytes 24580
  12.4 91.0 %copy-start.12 = (f32[128]{0:T(128)}, f32[128]{0:T(128)S(1)}, u32[]{:S(2)}) copy-start(f32[128]{0:T(128)S(1)} %broadcast_multiply_fusion.2) | copy-start | bytes 1540
  13.8 89.7 %copy-start.15 = (f32[128]{0:T(128)}, f32[128]{0:T(128)S(1)}, u32[]{:S(2)}) copy-start(f32[128]{0:T(128)S(1)} %add_rsqrt_fusion.1) | copy-start | bytes 1540
  103.4 86.3 %copy-start.1 = (bf16[1,128,2048]{2,1,0:T(8,128)(2,1)S(1)}, bf16[1,128,2048]{2,1,0:T(8,128)(2,1)}, u32[]{:S(2)}) copy-start(bf16[1,128,2048]{2,1,0:T(8,128)(2,1)} %param.10) | copy-start | bytes 1572868
  189.7 59.8 %copy-start.10 = (f32[2048]{0:T(1024)S(1)}, f32[2048]{0:T(1024)}, u32[]{:S(2)}) copy-start(f32[2048]{0:T(1024)} %copy-done.9) | copy-start | bytes 24580
  189.7 59.8 %copy-start.13 = (f32[128]{0:T(128)S(1)}, f32[128]{0:T(128)}, u32[]{:S(2)}) copy-start(f32[128]{0:T(128)} %copy-done.12) | copy-start | bytes 1540
  189.7 59.8 %copy-start.16 = (f32[128]{0:T(128)S(1)}, f32[128]{0:T(128)}, u32[]{:S(2)}) copy-start(f32[128]{0:T(128)} %copy-done.15) | copy-start | bytes 1540
  260.0 27.1 %copy-start.4 = (f32[16,64]{1,0:T(8,128)S(1)}, f32[16,64]{1,0:T(8,128)}, u32[]{:S(2)}) copy-start(f32[16,64]{1,0:T(8,128)} %get-tuple-element.2) | copy-start | bytes 12292
  260.2 25.1 %copy-start.14 = (u32[256]{0:T(256)S(1)}, u32[256]{0:T(256)}, u32[]{:S(2)}) copy-start(u32[256]{0:T(256)} %constant.88) | copy-start | bytes 3076
  260.2 25.7 %copy-start.11 = (bf16[1024]{0:T(1024)(128)(2,1)S(1)}, bf16[1024]{0:T(1024)(128)(2,1)}, u32[]{:S(2)}) copy-start(bf16[1024]{0:T(1024)(128)(2,1)} %param.18) | copy-start | bytes 6148
  261.2 29.4 %copy-start.6 = (f32[16,64]{1,0:T(8,128)S(1)}, f32[16,64]{1,0:T(8,128)}, u32[]{:S(2)}) copy-start(f32[16,64]{1,0:T(8,128)} %get-tuple-element.4) | copy-start | bytes 12292
  261.2 30.0 %copy-start.5 = (f32[16,64]{1,0:T(8,128)S(1)}, f32[16,64]{1,0:T(8,128)}, u32[]{:S(2)}) copy-start(f32[16,64]{1,0:T(8,128)} %get-tuple-element.5) | copy-start | bytes 12292
  261.2 30.6 %copy-start = (f32[2,64,16,64]{3,2,1,0:T(8,128)S(1)}, f32[2,64,16,64]{3,2,1,0:T(8,128)}, u32[]{:S(2)}) copy-start(f32[2,64,16,64]{3,2,1,0:T(8,128)} %get-tuple-element.13) | copy-start | bytes 1572868
  263.5 149.4 %all-reduce.6.cloned.1.call-start = ((), (), s32[]{:S(2)}) async-start(), calls=%async_computation.7 | async-start | bytes 131072
  280.6 206.0 %all-gather.12.cloned.1.call-start = ((), (), s32[]{:S(2)}) async-start(), calls=%async_computation.4 | async-start | bytes 4456448 | tf_op jit(solution)/shard_map/all_gather | solution.py:26
  283.2 294.4 %all-gather.14.cloned.1.call-start = ((), (), s32[]{:S(2)}) async-start(), calls=%async_computation.5 | async-start | bytes 4456448 | tf_op jit(solution)/shard_map/all_gather | solution.py:208
  290.6 4.7 copy-start.2
  291.8 194.8 %copy-start.8 = (f32[16,64]{1,0:T(8,128)S(1)}, f32[16,64]{1,0:T(8,128)}, u32[]{:S(2)}) copy-start(f32[16,64]{1,0:T(8,128)} %get-tuple-element.45) | copy-start | bytes 12292
  294.2 192.4 %copy-start.3 = (f32[2,64,16,64]{3,2,1,0:T(8,128)S(1)}, f32[2,64,16,64]{3,2,1,0:T(8,128)}, u32[]{:S(2)}) copy-start(f32[2,64,16,64]{3,2,1,0:T(8,128)} %get-tuple-element.16) | copy-start | bytes 1572868
  496.9 80.7 %copy-start.7 = (f32[1024]{0:T(1024)S(1)}, f32[1024]{0:T(1024)}, u32[]{:S(2)}) copy-start(f32[1024]{0:T(1024)} %convert_element_type.1001) | copy-start | bytes 12292
Sparse Core Ops, SparseCore 0:
  9.8 89.7 all-gather.9
  101.4 73.5 all-gather.7
  176.8 72.5 all-gather.5
  263.6 13.2 reduce-scatter.3
  280.7 132.1 all-reduce.5
  414.6 72.0 all-gather.11
  488.4 89.1 all-gather.13
where the time goes:
time: 589 us; the launch traced here: 588 us
  waiting for transfers between devices  400 us (68%)
  blocking collectives  107 us (18%)
  matrix products  31.4 us (5%)
  other arithmetic  18.4 us (3%)
  local copies, waits for them, and re-layouts  15.3 us (3%)
  between operations  15.2 us (3%)
    unnamed x8, waiting for transfers between devices  118 us
    all_gather x1, waiting for transfers between devices, body(): forget_sum = add_rows(lax.all_gather(w_forget, 'sp', axis=0, tiled=True))  85.1 us
    all_gather x1, waiting for transfers between devices, body(): lax.all_gather(w_output, 'sp', axis=1, tiled=True)  78.2 us
    all_gather x1, waiting for transfers between devices, entering_2(): lax.all_gather(part.astype(kind), axis)  63.5 us
    all_gather x5, blocking collectives, entering_2(): lax.all_gather(part.astype(kind), axis)  58.3 us
    all_gather x1, waiting for transfers between devices, body(): input_sum = add_rows(lax.all_gather(w_input, 'sp', axis=0, tiled=True))  55.5 us
    all_gather x3, blocking collectives, prefix_by_axis(): pieces = lax.all_gather(total, axis)  40.7 us
  transfers between devices with their start and end apart: 7, of which 5 were waited for; matrix products, arithmetic and copies ran while one was open for 8% of the time, Pallas kernels for 0%

commit v1 on v0

--- a/solution.py
+++ b/solution.py
@@ -9,6 +9,11 @@
 BLOCK = 64
 SP_TP = ("sp", "tp_0", "tp_1")
 EPSILON = 1e-05
+
+
+def gather_by_exchange(x, axis, dim):
+    copies = jnp.concatenate([x] * lax.axis_size(axis), axis=dim)
+    return lax.all_to_all(copies, axis, dim, dim, tiled=True)
 
 
 def nothing_yet(value, identity):
@@ -204,9 +209,7 @@
     )
     gated = scaled.reshape(seqs, span, HEADS * HEAD).astype(jnp.bfloat16)
     mixed = jnp.dot(
-        gated,
-        lax.all_gather(w_output, "sp", axis=1, tiled=True),
-        preferred_element_type=jnp.float32,
+        gated, gather_by_exchange(w_output, "sp", 1), preferred_element_type=jnp.float32
     ).astype(jnp.bfloat16)
     return (mixed, final_state)
 

time: 589 us -> 769 us (1.31)
  waiting for transfers between devices: 400 us -> 543 us
  starting transfers between devices: 0.44 us -> 24.5 us
  local copies, waits for them, and re-layouts: 15.3 us -> 30 us
    all_gather x1, waiting for transfers between devices: 85.1 us -> 221 us  [body(): forget_sum = add_rows(lax.all_gather(w_forget, 'sp', axis=0, tiled=True))]
    all_gather x1 -> x0, waiting for transfers between devices: 78.2 us -> none  [body(): lax.all_gather(w_output, 'sp', axis=1, tiled=True)]
    all_gather x1, waiting for transfers between devices: 0.01 us -> 72.4 us  [body(): query_sum = add_rows(lax.all_gather(w_query, 'sp', axis=0, tiled=True))]
    all_to_all x0 -> x1, starting transfers between devices: none -> 24.1 us  [gather_by_exchange(): return lax.all_to_all(copies, axis, dim, dim, tiled=True)]
    all_gather x1, waiting for transfers between devices: 55.5 us -> 70.5 us  [body(): input_sum = add_rows(lax.all_gather(w_input, 'sp', axis=0, tiled=True))]
    all_to_all x0 -> x2, local copies, waits for them, and re-layouts: none -> 12.9 us  [gather_by_exchange(): return lax.all_to_all(copies, axis, dim, dim, tiled=True)]
    unnamed x8 -> x7, waiting for transfers between devices: 118 us -> 116 us
where the time goes in v1:
time: 769 us; the launch traced here: 768 us
  waiting for transfers between devices  543 us (71%)
  blocking collectives  109 us (14%)
  matrix products  31.3 us (4%)
  local copies, waits for them, and re-layouts  30 us (4%)
  starting transfers between devices  24.5 us (3%)
  between operations  15.4 us (2%)
  other arithmetic  14.5 us (2%)
    all_gather x1, waiting for transfers between devices, body(): forget_sum = add_rows(lax.all_gather(w_forget, 'sp', axis=0, tiled=True))  221 us
    unnamed x7, waiting for transfers between devices  116 us
    all_gather x1, waiting for transfers between devices, body(): query_sum = add_rows(lax.all_gather(w_query, 'sp', axis=0, tiled=True))  72.4 us
    all_gather x1, waiting for transfers between devices, body(): input_sum = add_rows(lax.all_gather(w_input, 'sp', axis=0, tiled=True))  70.5 us
    all_gather x1, waiting for transfers between devices, entering_2(): lax.all_gather(part.astype(kind), axis)  63.4 us
    all_gather x5, blocking collectives, entering_2(): lax.all_gather(part.astype(kind), axis)  59.6 us
    all_gather x3, blocking collectives, prefix_by_axis(): pieces = lax.all_gather(total, axis)  40.7 us
    all_to_all x1, starting transfers between devices, gather_by_exchange(): return lax.all_to_all(copies, axis, dim, dim, tiled=True)  24.1 us
  transfers between devices with their start and end apart: 7, of which 5 were waited for; matrix products, arithmetic and copies ran while one was open for 8% of the time, Pallas kernels for 0%

profile of v1, /device:TPU:36, one launch (start us, length us, event | category | flops | bytes accessed | tf_op | source)
XLA Modules:
  0.0 767.8 jit_solution(6166079667572727115)
XLA Ops:
  13.0 6.4 copy.87
  19.5 24.1 %all-to-all-start = ((bf16[1024,16,128]{2,0,1:T(8,128)(2,1)}), bf16[1024,16,128]{2,0,1:T(8,128)(2,1)}, u32[]{:S(2)}, u32[]{:S(2)}) async-start(bf16[1024,16,128]{2,0,1:T(8,128)(2,1)} %copy.87), calls=%async_computation | async-start | bytes 8388608 | tf_op jit(solution)/shard_map/all_to_all | solution.py:16
  44.4 220.5 %all-gather.9.cloned.1.call-done = bf16[2048,1024]{1,0:T(8,128)(2,1)} async-done(((bf16[128,1024]{1,0:T(8,128)(2,1)}), bf16[2048,1024]{1,0:T(8,128)(2,1)}) %all-gather.9.cloned.1.call-update) | async-done | bytes 4194320 | tf_op jit(solution)/shard_map/all_gather | solution.py:156
  264.9 3.7 add_select_fusion
  270.2 72.4 %all-gather.7.cloned.1.call-done = bf16[2048,1024]{1,0:T(8,128)(2,1)} async-done(((bf16[128,1024]{1,0:T(8,128)(2,1)}), bf16[2048,1024]{1,0:T(8,128)(2,1)}) %all-gather.7.cloned.1.call-update) | async-done | bytes 4194320 | tf_op jit(solution)/shard_map/all_gather | solution.py:155
  342.6 3.0 divide_multiply_fusion.1
  346.8 70.5 %all-gather.5.cloned.1.call-done = bf16[2048,1024]{1,0:T(8,128)(2,1)} async-done(((bf16[128,1024]{1,0:T(8,128)(2,1)}), bf16[2048,1024]{1,0:T(8,128)(2,1)}) %all-gather.5.cloned.1.call-update) | async-done | bytes 4194320 | tf_op jit(solution)/shard_map/all_gather | solution.py:157
  417.4 2.9 convolution_convert_fusion.3
  425.5 10.8 %all_gather.49 = bf16[4,1,16,64]{3,2,1,0:T(8,128)(2,1)S(1)} all-gather(bf16[1,1,16,64]{3,2,1,0:T(8,128)(2,1)S(1)} %get-tuple-element.47), channel_id=1, replica_groups=mesh['grp'=2,'sp'=16,'tp_0'=4,'tp_1'=2] {'tp_0'}, dimensions={0}, use_global_device_ids=true | all-gather | bytes 10240 | tf_op jit(solution)/shard_map/all_gather | solution.py:31
  436.3 11.9 %all_gather.55 = f32[4,1,16,64]{3,2,1,0:T(8,128)S(1)} all-gather(f32[1,1,16,64]{3,2,1,0:T(8,128)S(1)} %slice_add_fusion.18), channel_id=1, replica_groups=mesh['grp'=2,'sp'=16,'tp_0'=4,'tp_1'=2] {'tp_0'}, dimensions={0}, use_global_device_ids=true | all-gather | bytes 20480 | tf_op jit(solution)/shard_map/all_gather | solution.py:51
  448.2 29.0 %all_gather.50 = bf16[16,1,16,64]{3,2,1,0:T(8,128)(2,1)S(1)} all-gather(bf16[1,1,16,64]{3,2,1,0:T(8,128)(2,1)S(1)} %get-tuple-element.37), channel_id=1, replica_groups=mesh['grp'=2,'sp'=16,'tp_0'=4,'tp_1'=2] {'sp'}, dimensions={0}, use_global_device_ids=true | all-gather | bytes 34816 | tf_op jit(solution)/shard_map/all_gather | solution.py:31
  477.3 26.9 %all_gather.56 = f32[16,1,16,64]{3,2,1,0:T(8,128)S(1)} all-gather(f32[1,1,16,64]{3,2,1,0:T(8,128)S(1)} %slice_add_fusion.15), channel_id=1, replica_groups=mesh['grp'=2,'sp'=16,'tp_0'=4,'tp_1'=2] {'sp'}, dimensions={0}, use_global_device_ids=true | all-gather | bytes 69632 | tf_op jit(solution)/shard_map/all_gather | solution.py:51
  505.3 3.3 fusion.16
  516.1 2.4 all_gather.51
  518.9 15.5 %all_gather.52 = bf16[4,1,16,64,64]{4,3,2,1,0:T(8,128)(2,1)} all-gather(bf16[1,1,16,64,64]{4,3,2,1,0:T(8,128)(2,1)S(1)} %fusion.36), channel_id=1, replica_groups=mesh['grp'=2,'sp'=16,'tp_0'=4,'tp_1'=2] {'tp_0'}, dimensions={0}, use_global_device_ids=true | all-gather | bytes 655360 | tf_op jit(solution)/shard_map/all_gather | solution.py:31
  534.5 2.5 fusion.52
  545.0 2.4 convolution_select_fusion
  548.4 3.0 fusion.1
  551.5 114.1 %all-reduce.6.cloned.1.call-done = bf16[64,1,512]{2,0,1:T(8,128)(2,1)} async-done(((bf16[64,1,512]{2,0,1:T(8,128)(2,1)}), bf16[64,1,512]{2,0,1:T(8,128)(2,1)}) %all-reduce.6.cloned.1.call-update) | async-done | bytes 65552
  666.3 8.5 %all-reduce.3 = bf16[4,1,512]{2,0,1:T(4,128)(2,1)S(1)} all-reduce(bf16[4,1,512]{2,0,1:T(4,128)(2,1)S(1)} %constant_dynamic-slice_fusion), channel_id=4, replica_groups=mesh['grp'=2,'sp'=16,'tp_0'=4,'tp_1'=2] {'tp_0'}, use_global_device_ids=true, to_apply=%region_6.7.clone | all-reduce | flops 2048 | bytes 8192
  675.9 63.4 %all-gather.11.cloned.1.call-done = bf16[16,1,16,64,64]{4,3,2,1,0:T(8,128)(2,1)} async-done(((bf16[1,1,16,64,64]{4,3,2,1,0:T(8,128)(2,1)}), bf16[16,1,16,64,64]{4,3,2,1,0:T(8,128)(2,1)}) %all-gather.11.cloned.1.call-update) | async-done | bytes 2097168 | tf_op jit(solution)/shard_map/all_gather | solution.py:31
  739.3 9.6 %multiply_reduce_fusion = (f32[2,64,16]{1,2,0:T(8,128)S(1)}, f32[1,2,64,16,64]{2,4,3,1,0:T(8,128)S(1)}) fusion(f32[1,2,64,16,64]{2,4,3,1,0:T(8,128)} %fusion.1, f32[2,64,16,64]{3,2,1,0:T(8,128)S(1)} %copy-done.4, f32[1,16,64,64]{3,2,1,0:T(8,128)} %param.17, bf16[16,1,16,64,64]{4,3,2,1,0:T(8,128)(2,1)} %all-gather.11.cloned.1.call-done, ...), kind=kOutput, calls=%fused_computation.34 | convolution fusion | flops 107018240 | bytes 4829206 | tf_op jit(solution)/shard_map/snthd,shde->snthe/dot_general | solution.py:133
  750.0 6.5 copy.88
  756.4 4.5 fusion
  (109 shorter events, 34.4 us)
Async XLA Ops:
  7.2 257.8 %all-gather.9.cloned.1.call-start = ((), (), s32[]{:S(2)}) async-start(), calls=%async_computation.4 | async-start | bytes 4456448 | tf_op jit(solution)/shard_map/all_gather | solution.py:156
  8.0 334.6 %all-gather.7.cloned.1.call-start = ((), (), s32[]{:S(2)}) async-start(), calls=%async_computation.3 | async-start | bytes 4456448 | tf_op jit(solution)/shard_map/all_gather | solution.py:155
  8.8 408.6 %all-gather.5.cloned.1.call-start = ((), (), s32[]{:S(2)}) async-start(), calls=%async_computation.2 | async-start | bytes 4456448 | tf_op jit(solution)/shard_map/all_gather | solution.py:157
  11.1 1.9 copy-start
  19.5 24.3 %copy-start.8 = (bf16[2048]{0:T(1024)(128)(2,1)S(1)}, bf16[2048]{0:T(1024)(128)(2,1)}, u32[]{:S(2)}) copy-start(bf16[2048]{0:T(1024)(128)(2,1)} %param.11) | copy-start | bytes 12292
  19.5 24.3 %copy-start.5 = (f32[1,128,16]{1,2,0:T(8,128)S(1)}, f32[1,128,16]{1,2,0:T(8,128)}, u32[]{:S(2)}) copy-start(f32[1,128,16]{1,2,0:T(8,128)} %param.16) | copy-start | bytes 24580
  19.5 24.4 %copy-start.2 = (bf16[1,128,2048]{2,1,0:T(8,128)(2,1)S(1)}, bf16[1,128,2048]{2,1,0:T(8,128)(2,1)}, u32[]{:S(2)}) copy-start(bf16[1,128,2048]{2,1,0:T(8,128)(2,1)} %param.10) | copy-start | bytes 1572868
  19.5 24.9 %copy-start.9 = (f32[1024]{0:T(1024)S(1)}, f32[1024]{0:T(1024)}, u32[]{:S(2)}) copy-start(f32[1024]{0:T(1024)} %param.15) | copy-start | bytes 12292
  19.5 730.4 %all-to-all-start = ((bf16[1024,16,128]{2,0,1:T(8,128)(2,1)}), bf16[1024,16,128]{2,0,1:T(8,128)(2,1)}, u32[]{:S(2)}, u32[]{:S(2)}) async-start(bf16[1024,16,128]{2,0,1:T(8,128)(2,1)} %copy.87), calls=%async_computation | async-start | bytes 8388608 | tf_op jit(solution)/shard_map/all_to_all | solution.py:16
  43.6 490.7 %reduce-scatter.4.cloned.1.call-start = ((), (), s32[]{:S(2)}) async-start(), calls=%async_computation.6 | async-start | bytes 196608 | tf_op jit(solution)/shard_map/reduce_scatter | solution.py:66
  511.8 25.2 %copy-start.10 = (bf16[1024]{0:T(1024)(128)(2,1)S(1)}, bf16[1024]{0:T(1024)(128)(2,1)}, u32[]{:S(2)}) copy-start(bf16[1024]{0:T(1024)(128)(2,1)} %param.18) | copy-start | bytes 6148
  511.8 26.5 %copy-start.11 = (u32[256]{0:T(256)S(1)}, u32[256]{0:T(256)}, u32[]{:S(2)}) copy-start(u32[256]{0:T(256)} %constant.88) | copy-start | bytes 3076
  513.7 31.2 %copy-start.1 = (f32[2,64,16,64]{3,2,1,0:T(8,128)S(1)}, f32[2,64,16,64]{3,2,1,0:T(8,128)}, u32[]{:S(2)}) copy-start(f32[2,64,16,64]{3,2,1,0:T(8,128)} %get-tuple-element.13) | copy-start | bytes 1572868
  516.0 149.5 %all-reduce.6.cloned.1.call-start = ((), (), s32[]{:S(2)}) async-start(), calls=%async_computation.7 | async-start | bytes 131072
  534.5 204.8 %all-gather.11.cloned.1.call-start = ((), (), s32[]{:S(2)}) async-start(), calls=%async_computation.5 | async-start | bytes 4456448 | tf_op jit(solution)/shard_map/all_gather | solution.py:31
  544.9 3.5 copy-start.3
  544.9 194.4 %copy-start.6 = (f32[16,64]{1,0:T(8,128)S(1)}, f32[16,64]{1,0:T(8,128)}, u32[]{:S(2)}) copy-start(f32[16,64]{1,0:T(8,128)} %get-tuple-element.45) | copy-start | bytes 12292
  545.0 194.4 %copy-start.7 = (f32[16,64]{1,0:T(8,128)S(1)}, f32[16,64]{1,0:T(8,128)}, u32[]{:S(2)}) copy-start(f32[16,64]{1,0:T(8,128)} %exp.349) | copy-start | bytes 12292
  547.4 191.9 %copy-start.4 = (f32[2,64,16,64]{3,2,1,0:T(8,128)S(1)}, f32[2,64,16,64]{3,2,1,0:T(8,128)}, u32[]{:S(2)}) copy-start(f32[2,64,16,64]{3,2,1,0:T(8,128)} %get-tuple-element.16) | copy-start | bytes 1572868
Sparse Core Ops, SparseCore 0:
  9.8 255.0 all-gather.8
  266.8 75.7 all-gather.6
  344.4 72.9 all-gather.4
  516.2 13.4 reduce-scatter.3
  534.6 130.9 all-reduce.5
  667.2 72.0 all-gather.10
